TPU v7x, 32 devices: a whole 2x2x4 slice. The times are simulated.
32 devices in a mesh: ep: 8 (over z, x), tp: 4 (over y, core).
Axes of the slice: x: 2, y: 2, z: 4, core: 2. Of those that a mesh axis runs over, the one named last changes fastest.
Arguments:
- tokens: bfloat16 [128, 2048], P('ep'), may hold values from -6 to 6
- lengths: int32 [128], P('ep'), may hold values from 1024 to 16384
- old_state: float32 [128, 8, 128, 128], P('ep', 'tp'), may hold values from -2 to 2
- query_weight: bfloat16 [2048, 1024], P(None, 'tp'), may hold values from -0.125 to 0.125
- key_weight: bfloat16 [2048, 1024], P(None, 'tp'), may hold values from -0.125 to 0.125
- value_weight: bfloat16 [2048, 1024], P(None, 'tp'), may hold values from -0.125 to 0.125
- gate_weight: bfloat16 [2048, 1024], P(None, 'tp'), may hold values from -0.125 to 0.125
- head_gain: float32 [1024], P('tp'), may hold values from 0.1 to 1.9
- output_weight: bfloat16 [1024, 2048], P('tp'), may hold values from -0.1875 to 0.1875
- first_gain: float32 [2048], replicated, may hold values from 0.1 to 1.9
- expert_ids: int32 [128, 6], P('ep'), may hold values from 0 to 15, all different within a row; in each aligned block of 16 rows (0 to 15, 16 to 31, ...) at most 7 rows name the same one
- expert_weights: float32 [128, 6], P('ep'), may hold values from 0.05 to 0.8
- expert_gate: bfloat16 [16, 2048, 512], P('ep', None, 'tp'), may hold values from -0.125 to 0.125
- expert_up: bfloat16 [16, 2048, 512], P('ep', None, 'tp'), may hold values from -0.125 to 0.125
- expert_down: bfloat16 [16, 512, 2048], P('ep', 'tp'), may hold values from -0.25 to 0.25
- shared_gate: bfloat16 [2048, 512], P(None, 'tp'), may hold values from -0.125 to 0.125
- shared_up: bfloat16 [2048, 512], P(None, 'tp'), may hold values from -0.125 to 0.125
- shared_down: bfloat16 [512, 2048], P('tp'), may hold values from -0.25 to 0.25
- side_gate: bfloat16 [2048], replicated, may hold values from -0.125 to 0.125
- dense_gate: bfloat16 [2048, 8192], P(None, ('ep', 'tp')), may hold values from -0.125 to 0.125
- dense_up: bfloat16 [2048, 8192], P(None, ('ep', 'tp')), may hold values from -0.125 to 0.125
- dense_down: bfloat16 [8192, 2048], P(('ep', 'tp')), may hold values from -0.25 to 0.25
- second_gain: float32 [2048], replicated, may hold values from 0.1 to 1.9
Outputs:
- layer_out: bfloat16 [128, 2048], P('ep')
- new_state: float32 [128, 8, 128, 128], P('ep', 'tp')
Inputs may be any that keep to these rules, and one draw needn't show every extreme that they name: `expert_ids`: each row names 6 different experts. Among the 16 rows of one index of ep no expert is named by more than 7 rows, a bound that some block reaches.
All inputs are finite; a program needn't handle non-finite values.
Results may differ from a plain program's by a relative error of at most 0.017.
Values may be sent and summed in bfloat16 or wider, within the bound.
A program may use at most 64 MiB of HBM per device.

v0:
```python
import jax
import jax.numpy as jnp
from jax import lax
from jax.sharding import PartitionSpec as P

HEADS = 8
NORM_EPS = 1e-05
RESIDUAL_SCALE = 2.0**0.5


def rotate(inputs, positions):
    half_size = inputs.shape[-1] // 2
    frequency = 1.0 / 10000.0 ** (jnp.arange(half_size, dtype=jnp.float32) * 2.0 / inputs.shape[-1])
    angles = positions.astype(jnp.float32)[:, None] * frequency[None, :]
    cosine = jnp.cos(angles)[:, None, :]
    sine_part = jnp.sin(angles)[:, None, :]
    first_half = inputs[..., :half_size]
    second_half = inputs[..., half_size:]
    return jnp.concatenate(
        [
            first_half * cosine - second_half * sine_part,
            first_half * sine_part + second_half * cosine,
        ],
        axis=-1,
    )


def layer_norm(inputs, scale_gain):
    average = jnp.mean(inputs, axis=-1, keepdims=True)
    centered = inputs - average
    variance = jnp.mean(centered * centered, axis=-1, keepdims=True)
    return centered * lax.rsqrt(variance + NORM_EPS) * scale_gain


def expert_partial(arrived, expert_gate, expert_up, expert_down):
    gate_part = jnp.einsum(
        "secd,edf->secf", arrived, expert_gate, preferred_element_type=jnp.float32
    )
    up_part = jnp.einsum("secd,edf->secf", arrived, expert_up, preferred_element_type=jnp.float32)
    hidden = (jax.nn.silu(gate_part) * up_part).astype(jnp.bfloat16)
    return jnp.einsum("secf,efd->secd", hidden, expert_down, preferred_element_type=jnp.float32)


def route_experts(after_mixer, expert_ids, expert_weights, expert_gate, expert_up, expert_down):
    row_count, model_width = after_mixer.shape
    top_count = expert_ids.shape[1]
    local_experts = expert_gate.shape[0]
    ep_size = lax.axis_size("ep")
    tp_size = lax.axis_size("tp")
    total_experts = local_experts * ep_size
    capacity = max(2, row_count * top_count // total_experts + 1)
    flat_ids = expert_ids.reshape(-1)
    onehot = (flat_ids[:, None] == jnp.arange(total_experts, dtype=jnp.int32)[None, :]).astype(
        jnp.int32
    )
    slot_rank = jnp.sum(onehot * (jnp.cumsum(onehot, axis=0) - 1), axis=1)
    targets = flat_ids * capacity + slot_rank
    placing = (
        jnp.arange(total_experts * capacity, dtype=jnp.int32)[:, None] == targets[None, :]
    ).astype(jnp.bfloat16)
    repeated = jnp.repeat(after_mixer, top_count, axis=0)
    outgoing = jnp.dot(placing, repeated, preferred_element_type=jnp.float32).astype(jnp.bfloat16)
    outgoing = outgoing.reshape(ep_size, local_experts, capacity, model_width)
    column_width = model_width // tp_size
    own_cols = lax.dynamic_slice_in_dim(
        outgoing, lax.axis_index("tp") * column_width, column_width, 3
    )
    arrived = lax.all_to_all(own_cols, "ep", split_axis=0, concat_axis=0, tiled=True)
    whole_rows = lax.all_gather(arrived, "tp", axis=3, tiled=True)
    outputs = expert_partial(whole_rows, expert_gate, expert_up, expert_down)
    reduced = lax.psum_scatter(outputs.astype(jnp.bfloat16), "tp", scatter_dimension=3, tiled=True)
    came_back = lax.all_to_all(reduced, "ep", split_axis=0, concat_axis=0, tiled=True)
    returned = lax.all_gather(came_back, "tp", axis=3, tiled=True)
    returned = returned.reshape(total_experts * capacity, model_width)
    gathered_back = jnp.dot(placing.T, returned, preferred_element_type=jnp.float32)
    weighted = gathered_back.reshape(row_count, top_count, model_width) * expert_weights[:, :, None]
    return jnp.sum(weighted, axis=1)


def side_branch(
    after_mixer, shared_gate, shared_up, shared_down, side_gate, dense_gate, dense_up, dense_down
):
    row_count = after_mixer.shape[0]
    row_piece = lax.all_gather(after_mixer, "ep", axis=0, tiled=True)
    switch = jax.nn.sigmoid(jnp.dot(row_piece, side_gate, preferred_element_type=jnp.float32))
    gate_part = jnp.dot(row_piece, dense_gate, preferred_element_type=jnp.float32)
    up_part = jnp.dot(row_piece, dense_up, preferred_element_type=jnp.float32)
    dense_hidden = (jax.nn.silu(gate_part) * up_part * switch[:, None]).astype(jnp.bfloat16)
    shared_hidden = (
        jax.nn.silu(jnp.dot(after_mixer, shared_gate, preferred_element_type=jnp.float32))
        * jnp.dot(after_mixer, shared_up, preferred_element_type=jnp.float32)
    ).astype(jnp.bfloat16)
    total_rows = dense_hidden.shape[0]
    placed = lax.dynamic_update_slice_in_dim(
        jnp.zeros((total_rows, shared_hidden.shape[1]), jnp.bfloat16),
        shared_hidden,
        lax.axis_index("ep") * row_count,
        0,
    )
    hidden_all = jnp.concatenate([dense_hidden, placed], axis=1)
    down_all = jnp.concatenate([dense_down, shared_down], axis=0)
    own_rows = lax.psum_scatter(
        jnp.dot(hidden_all, down_all, preferred_element_type=jnp.float32),
        ("ep", "tp"),
        scatter_dimension=0,
        tiled=True,
    )
    return lax.all_gather(own_rows.astype(jnp.bfloat16), "tp", axis=0, tiled=True)


def per_device(
    tokens,
    lengths,
    old_state,
    query_weight,
    key_weight,
    value_weight,
    gate_weight,
    head_gain,
    output_weight,
    first_gain,
    expert_ids,
    expert_weights,
    expert_gate,
    expert_up,
    expert_down,
    shared_gate,
    shared_up,
    shared_down,
    side_gate,
    dense_gate,
    dense_up,
    dense_down,
    second_gain,
):
    row_count = tokens.shape[0]
    local_heads = old_state.shape[1]
    head_size = old_state.shape[-1]
    queries = jnp.dot(tokens, query_weight, preferred_element_type=jnp.float32).reshape(
        row_count, local_heads, head_size
    )
    keys_raw = jnp.dot(tokens, key_weight, preferred_element_type=jnp.float32).reshape(
        row_count, local_heads, head_size
    )
    keys_raw = keys_raw * head_size ** (-0.5)
    values = jnp.dot(tokens, value_weight, preferred_element_type=jnp.float32).reshape(
        row_count, local_heads, head_size
    )
    gating = jnp.dot(tokens, gate_weight, preferred_element_type=jnp.float32)
    query_rot = rotate(queries, lengths)
    key_rot = rotate(keys_raw, lengths)
    head_ids = (
        lax.axis_index("tp") * local_heads + jnp.arange(local_heads, dtype=jnp.int32)
    ).astype(jnp.float32)
    decays = 1.0 - jnp.exp2(-2.0 - 10.0 * head_ids / (HEADS - 1))
    new_state = (
        decays[None, :, None, None] * old_state + key_rot[:, :, :, None] * values[:, :, None, :]
    )
    readout = jnp.einsum("thi,thij->thj", query_rot, new_state, precision=lax.Precision.HIGHEST)
    normed = layer_norm(readout, head_gain.reshape(local_heads, head_size))
    mixed = (normed.reshape(row_count, local_heads * head_size) * jax.nn.silu(gating)).astype(
        jnp.bfloat16
    )
    partial_value = jnp.dot(mixed, output_weight, preferred_element_type=jnp.float32)
    branch = lax.psum(partial_value.astype(jnp.bfloat16), "tp").astype(jnp.float32)
    after_mixer = layer_norm(
        RESIDUAL_SCALE * tokens.astype(jnp.float32) + branch, first_gain
    ).astype(jnp.bfloat16)
    routed = route_experts(
        after_mixer, expert_ids, expert_weights, expert_gate, expert_up, expert_down
    )
    side = side_branch(
        after_mixer,
        shared_gate,
        shared_up,
        shared_down,
        side_gate,
        dense_gate,
        dense_up,
        dense_down,
    )
    total = RESIDUAL_SCALE * after_mixer.astype(jnp.float32) + routed + side.astype(jnp.float32)
    layer_out = layer_norm(total, second_gain).astype(jnp.bfloat16)
    return (layer_out, new_state)


def solution(mesh):
    return jax.shard_map(
        per_device,
        mesh=mesh,
        in_specs=(
            P("ep", None),
            P("ep"),
            P("ep", "tp", None, None),
            P(None, "tp"),
            P(None, "tp"),
            P(None, "tp"),
            P(None, "tp"),
            P("tp"),
            P("tp", None),
            P(),
            P("ep", None),
            P("ep", None),
            P("ep", None, "tp"),
            P("ep", None, "tp"),
            P("ep", "tp", None),
            P(None, "tp"),
            P(None, "tp"),
            P("tp", None),
            P(),
            P(None, ("ep", "tp")),
            P(None, ("ep", "tp")),
            P(("ep", "tp"), None),
            P(),
        ),
        out_specs=(P("ep", None), P("ep", "tp", None, None)),
        check_vma=False,
    )
```

profile of v0, /device:TPU:0, one launch (start us, length us, event | category | flops | bytes accessed | tf_op | source)
XLA Modules:
  0.0 191.7 jit_solution(2164469225561733974)
XLA Ops:
  7.3 1.6 convolution_multiply_fusion.2
  8.9 0.7 convert_element_type.61
  9.6 1.5 fusion.43
  11.1 0.2 fusion.44
  11.4 0.1 multiply_cosine_fusion
  11.5 0.1 multiply_subtract_fusion
  11.7 0.1 pad_maximum_fusion
  11.8 2.0 %multiply_add_fusion = f32[16,2,128,128]{3,2,1,0:T(8,128)S(1)} fusion(f32[16,2,128,128]{3,2,1,0:T(8,128)} %param.25, f32[16,2,128]{2,1,0:T(2,128)S(1)} %mul.268, f32[16,2,128]{2,1,0:T(2,128)S(1)} %get-tuple-element.13, f32[2]{0:T(128)S(1)} %exponential_subtract_fusion), kind=kLoop, calls=%fused_computation.5 | loop fusion | flops 1572864 | bytes 4227080 | tf_op jit(solution)/shard_map/add | solution.py:157
  13.8 1.9 fusion.45
  15.7 0.1 reduce_sum.72
  15.8 0.2 multiply_reduce_fusion.2
  16.0 0.1 multiply_multiply_fusion
  16.1 2.9 %convolution_convert_fusion.2 = bf16[16,2048]{1,0:T(8,128)(2,1)} fusion(bf16[256,2048]{1,0:T(8,128)(2,1)} %param.31, f32[2,8,2,128]{3,2,1,0:T(2,128)S(1)} %bitcast.80, bf16[16,2048]{1,0:T(8,128)(2,1)S(1)} %copy-done.2, bf16[2048,256]{1,0:T(8,128)(2,1)} %param.29), kind=kOutput, calls=%fused_computation.4 | convolution fusion | flops 33611776 | bytes 2244608 | tf_op jit(solution)/shard_map/dot_general | solution.py:164
  19.1 0.1 reshape.166
  19.3 0.1 reduce_window_sum.11
  19.4 0.2 select_reduce_fusion
  19.8 33.6 %all-reduce.4.cloned.1.call-done = bf16[16,2048]{1,0:T(8,128)(2,1)} async-done(((bf16[16,2048]{1,0:T(8,128)(2,1)}), bf16[16,2048]{1,0:T(8,128)(2,1)}) %all-reduce.4.cloned.1.call-update) | async-done | bytes 65552 | tf_op jit(solution)/shard_map/psum | solution.py:165
  53.4 1.0 fusion.20
  54.4 1.0 multiply_reduce_fusion.1
  55.5 0.9 multiply_convert_fusion.1
  56.4 31.4 %all_gather.14 = bf16[128,2048]{1,0:T(8,128)(2,1)S(1)} all-gather(bf16[16,2048]{1,0:T(8,128)(2,1)S(1)} %multiply_convert_fusion.1), channel_id=1, replica_groups=mesh['ep'=8,'tp'=4] {'ep'}, dimensions={0}, use_global_device_ids=true | all-gather | bytes 589824 | tf_op jit(solution)/shard_map/all_gather | solution.py:84
  87.8 1.2 fusion.47
  89.1 0.1 reshape.167
  89.2 0.3 convolution_convert_fusion
  89.5 0.2 reshape.168
  89.7 0.7 copy.36
  90.4 5.3 %all-to-all-start = ((bf16[8,2,7,512]{3,1,2,0:T(2,128)(2,1)}), bf16[8,2,7,512]{3,1,2,0:T(2,128)(2,1)S(1)}, u32[]{:S(2)}, u32[]{:S(2)}) async-start(bf16[8,2,7,512]{3,1,2,0:T(2,128)(2,1)} %copy.36), calls=%async_computation | async-start | bytes 229376 | tf_op jit(solution)/shard_map/all_to_all | solution.py:68
  95.8 1.6 fusion.46
  97.5 0.2 fusion.11
  97.7 5.3 %all-to-all-done = bf16[8,2,7,512]{3,1,2,0:T(2,128)(2,1)S(1)} async-done(((bf16[8,2,7,512]{3,1,2,0:T(2,128)(2,1)}), bf16[8,2,7,512]{3,1,2,0:T(2,128)(2,1)S(1)}, u32[]{:S(2)}, u32[]{:S(2)}) %all-to-all-start) | async-done | bytes 114720 | tf_op jit(solution)/shard_map/all_to_all | solution.py:68
  103.0 6.3 %all_gather.12 = bf16[8,2,7,2048]{3,0,2,1:T(8,128)(2,1)S(1)} all-gather(bf16[8,2,7,512]{3,0,2,1:T(8,128)(2,1)S(1)} %copy.37), channel_id=1, replica_groups=mesh['ep'=8,'tp'=4] {'tp'}, dimensions={3}, use_global_device_ids=true | all-gather | bytes 573440 | tf_op jit(solution)/shard_map/all_gather | solution.py:69
  109.3 1.5 convolution_bitcast_fusion.1
  110.9 1.3 fusion
  112.2 0.2 fusion.15
  112.4 1.7 fusion.7
  114.2 0.4 fusion.1
  114.6 49.3 %all-reduce.5 = bf16[128,2048]{1,0:T(8,128)(2,1)S(1)} all-reduce(f32[128,2048]{1,0:T(8,128)S(1)} %fusion.1), channel_id=3, replica_groups=mesh['ep'=8,'tp'=4] {'ep','tp'}, use_global_device_ids=true, to_apply=%region_9.10.clone | all-reduce | flops 262144 | bytes 1572864
  164.0 1.6 copy.38
  165.6 3.7 %all-to-all-start.1 = ((bf16[8,2,7,512]{3,1,2,0:T(2,128)(2,1)}), bf16[8,2,7,512]{3,1,2,0:T(2,128)(2,1)S(1)}, u32[]{:S(2)}, u32[]{:S(2)}) async-start(bf16[8,2,7,512]{3,1,2,0:T(2,128)(2,1)} %copy.38), calls=%async_computation.2 | async-start | bytes 229376 | tf_op jit(solution)/shard_map/all_to_all | solution.py:72
  169.4 5.2 %all-gather = bf16[4,4,2048]{2,1,0:T(4,128)(2,1)S(1)} all-gather(bf16[1,4,2048]{2,1,0:T(4,128)(2,1)S(1)} %fusion.33), channel_id=1, replica_groups=mesh['ep'=8,'tp'=4] {'tp'}, dimensions={0}, use_global_device_ids=true | all-gather | bytes 81920 | tf_op jit(solution)/shard_map/all_gather | solution.py:108
  174.6 2.0 %all-to-all-done.1 = bf16[8,2,7,512]{3,1,2,0:T(2,128)(2,1)S(1)} async-done(((bf16[8,2,7,512]{3,1,2,0:T(2,128)(2,1)}), bf16[8,2,7,512]{3,1,2,0:T(2,128)(2,1)S(1)}, u32[]{:S(2)}, u32[]{:S(2)}) %all-to-all-start.1) | async-done | bytes 114720 | tf_op jit(solution)/shard_map/all_to_all | solution.py:72
  176.6 6.6 %all_gather.13 = bf16[8,2,7,2048]{3,1,2,0:T(2,128)(2,1)S(1)} all-gather(bf16[8,2,7,512]{3,1,2,0:T(2,128)(2,1)S(1)} %all-to-all-done.1), channel_id=1, replica_groups=mesh['ep'=8,'tp'=4] {'tp'}, dimensions={3}, use_global_device_ids=true | all-gather | bytes 573440 | tf_op jit(solution)/shard_map/all_gather | solution.py:73
  183.2 0.2 copy.39
  183.3 0.2 reshape.178
  183.5 0.3 fusion.5
  183.8 0.1 fusion.40
  183.9 0.2 multiply_reduce_fusion
  184.2 0.7 multiply_convert_fusion
  (60 shorter events, 0.8 us)
Async XLA Ops:
  7.2 103.7 %copy-start = (bf16[2,128,2048]{2,1,0:T(8,128)(2,1)S(1)}, bf16[2,128,2048]{2,1,0:T(8,128)(2,1)}, u32[]{:S(2)}) copy-start(bf16[2,128,2048]{2,1,0:T(8,128)(2,1)} %param.37) | copy-start | bytes 3145732
  7.2 3.9 %copy-start.2 = (bf16[16,2048]{1,0:T(8,128)(2,1)S(1)}, bf16[16,2048]{1,0:T(8,128)(2,1)}, u32[]{:S(2)}) copy-start(bf16[16,2048]{1,0:T(8,128)(2,1)} %param.23) | copy-start | bytes 196612
  7.2 3.9 %copy-start.4 = (bf16[2048,256]{1,0:T(8,128)(2,1)S(1)}, bf16[2048,256]{1,0:T(8,128)(2,1)}, u32[]{:S(2)}) copy-start(bf16[2048,256]{1,0:T(8,128)(2,1)} %param.28) | copy-start | bytes 3145732
  7.2 46.2 %all-reduce.4.cloned.1.call-start = ((), (), s32[]{:S(2)}) async-start(), calls=%async_computation.3 | async-start | bytes 131072 | tf_op jit(solution)/shard_map/psum | solution.py:165
  13.7 5.3 %copy-start.1 = (f32[16,2,128,128]{3,2,1,0:T(8,128)}, f32[16,2,128,128]{3,2,1,0:T(8,128)S(1)}, u32[]{:S(2)}) copy-start(f32[16,2,128,128]{3,2,1,0:T(8,128)S(1)} %multiply_add_fusion) | copy-start | bytes 6291460
  13.7 2.2 %copy-start.12 = (f32[256]{0:T(256)S(1)}, f32[256]{0:T(256)}, u32[]{:S(2)}) copy-start(f32[256]{0:T(256)} %param.30) | copy-start | bytes 3076
  13.8 5.3 %copy-start.10 = (s32[16,6]{0,1:T(8,128)S(1)}, s32[16,6]{0,1:T(8,128)}, u32[]{:S(2)}) copy-start(s32[16,6]{0,1:T(8,128)} %param.33) | copy-start | bytes 1156
  13.8 6.0 %copy-start.11 = (bf16[2048]{0:T(1024)(128)(2,1)S(1)}, bf16[2048]{0:T(1024)(128)(2,1)}, u32[]{:S(2)}) copy-start(bf16[2048]{0:T(1024)(128)(2,1)} %param.41) | copy-start | bytes 12292
  13.8 41.7 %copy-start.8 = (f32[2048]{0:T(1024)S(1)}, f32[2048]{0:T(1024)}, u32[]{:S(2)}) copy-start(f32[2048]{0:T(1024)} %param.32) | copy-start | bytes 24580
  89.2 8.2 %copy-start.5 = (bf16[2048,128]{1,0:T(8,128)(2,1)S(1)}, bf16[2048,128]{1,0:T(8,128)(2,1)}, u32[]{:S(2)}) copy-start(bf16[2048,128]{1,0:T(8,128)(2,1)} %param.39) | copy-start | bytes 1572868
  90.4 12.6 %all-to-all-start = ((bf16[8,2,7,512]{3,1,2,0:T(2,128)(2,1)}), bf16[8,2,7,512]{3,1,2,0:T(2,128)(2,1)S(1)}, u32[]{:S(2)}, u32[]{:S(2)}) async-start(bf16[8,2,7,512]{3,1,2,0:T(2,128)(2,1)} %copy.36), calls=%async_computation | async-start | bytes 229376 | tf_op jit(solution)/shard_map/all_to_all | solution.py:68
  95.8 15.1 %copy-start.3 = (bf16[2,2048,128]{2,1,0:T(8,128)(2,1)S(1)}, bf16[2,2048,128]{2,1,0:T(8,128)(2,1)}, u32[]{:S(2)}) copy-start(bf16[2,2048,128]{2,1,0:T(8,128)(2,1)} %param.36) | copy-start | bytes 3145732
  95.8 68.2 %reduce-scatter.2.cloned.1.call-start = ((), (), s32[]{:S(2)}) async-start(), calls=%async_computation.4 | async-start | bytes 573440 | tf_op jit(solution)/shard_map/reduce_scatter | solution.py:71
  97.6 5.4 %copy-start.6 = (bf16[128,128]{1,0:T(8,128)(2,1)}, bf16[128,128]{1,0:T(8,128)(2,1)S(1)}, u32[]{:S(2)}) copy-start(bf16[128,128]{1,0:T(8,128)(2,1)S(1)} %fusion.11) | copy-start | bytes 98308
  112.2 2.0 %copy-start.7 = (bf16[128,128]{1,0:T(8,128)(2,1)S(1)}, bf16[128,128]{1,0:T(8,128)(2,1)}, u32[]{:S(2)}) copy-start(bf16[128,128]{1,0:T(8,128)(2,1)} %copy-done.6) | copy-start | bytes 98308
  112.2 2.0 %copy-start.13 = (bf16[256,2048]{1,0:T(8,128)(2,1)S(1)}, bf16[256,2048]{1,0:T(8,128)(2,1)}, u32[]{:S(2)}) copy-start(bf16[256,2048]{1,0:T(8,128)(2,1)} %param.44) | copy-start | bytes 3145732
  112.2 2.0 %copy-start.14 = (bf16[128,2048]{1,0:T(8,128)(2,1)S(1)}, bf16[128,2048]{1,0:T(8,128)(2,1)}, u32[]{:S(2)}) copy-start(bf16[128,2048]{1,0:T(8,128)(2,1)} %param.40) | copy-start | bytes 1572868
  114.6 68.9 %copy-start.15 = (f32[16,6]{0,1:T(8,128)S(1)}, f32[16,6]{0,1:T(8,128)}, u32[]{:S(2)}) copy-start(f32[16,6]{0,1:T(8,128)} %param.34) | copy-start | bytes 1156
  165.6 11.0 %all-to-all-start.1 = ((bf16[8,2,7,512]{3,1,2,0:T(2,128)(2,1)}), bf16[8,2,7,512]{3,1,2,0:T(2,128)(2,1)S(1)}, u32[]{:S(2)}, u32[]{:S(2)}) async-start(bf16[8,2,7,512]{3,1,2,0:T(2,128)(2,1)} %copy.38), calls=%async_computation.2 | async-start | bytes 229376 | tf_op jit(solution)/shard_map/all_to_all | solution.py:72
  169.3 14.8 %copy-start.9 = (f32[2048]{0:T(1024)S(1)}, f32[2048]{0:T(1024)}, u32[]{:S(2)}) copy-start(f32[2048]{0:T(1024)} %param.45) | copy-start | bytes 24580
Sparse Core Ops, SparseCore 0:
  19.1 34.2 all-reduce.3
  112.3 18.7 reduce-scatter.1
where the time goes:
time: 192 us
  blocking collectives  98.9 us (52%)
  waiting for transfers between devices  41 us (21%)
  matrix products  16.9 us (9%)
  between operations  14.6 us (8%)
  starting transfers between devices  9.12 us (5%)
  other arithmetic  7.84 us (4%)
  local copies, waits for them, and re-layouts  3.44 us (2%)
    unnamed x1, blocking collectives  49.3 us
    psum x1, waiting for transfers between devices, per_device(): lax.psum(partial_value.astype(jnp.bfloat16), 'tp').astype(jnp.float32)  33.6 us
    all_gather x1, blocking collectives, side_branch(): row_piece = lax.all_gather(after_mixer, 'ep', axis=0, tiled=True)  31.4 us
    all_gather x1, blocking collectives, route_experts(): returned = lax.all_gather(came_back, 'tp', axis=3, tiled=True)  6.6 us
    all_gather x1, blocking collectives, route_experts(): whole_rows = lax.all_gather(arrived, 'tp', axis=3, tiled=True)  6.32 us
    all_to_all x1, waiting for transfers between devices, route_experts(): lax.all_to_all(own_cols, 'ep', split_axis=0, concat_axis=0, tiled=True)  5.33 us
    all_to_all x1, starting transfers between devices, route_experts(): lax.all_to_all(own_cols, 'ep', split_axis=0, concat_axis=0, tiled=True)  5.32 us
    all_gather x1, blocking collectives, side_branch(): lax.all_gather(own_rows.astype(jnp.bfloat16), 'tp', axis=0, tiled=True)  5.24 us
  transfers between devices with their start and end apart: 4, of which 3 were waited for; matrix products, arithmetic and copies ran while one was open for 3% of the time, Pallas kernels for 0%

commit v1 on v0

--- a/solution.py
+++ b/solution.py
@@ -162,7 +162,9 @@
         jnp.bfloat16
     )
     partial_value = jnp.dot(mixed, output_weight, preferred_element_type=jnp.float32)
-    branch = lax.psum(partial_value.astype(jnp.bfloat16), "tp").astype(jnp.float32)
+    branch = jnp.sum(lax.all_gather(partial_value.astype(jnp.bfloat16), "tp"), axis=0).astype(
+        jnp.float32
+    )
     after_mixer = layer_norm(
         RESIDUAL_SCALE * tokens.astype(jnp.float32) + branch, first_gain
     ).astype(jnp.bfloat16)

time: 192 us -> 167 us (0.87)
  waiting for transfers between devices: 41 us -> 7.18 us
  blocking collectives: 98.9 us -> 109 us
  other arithmetic: 7.84 us -> 5.35 us
    psum x1 -> x0, waiting for transfers between devices: 33.6 us -> none  [per_device(): lax.psum(partial_value.astype(jnp.bfloat16), 'tp').astype(jnp.float32)]
    all_gather x0 -> x1, blocking collectives: none -> 7.26 us  [per_device(): lax.all_gather(partial_value.astype(jnp.bfloat16), 'tp')]
    all_to_all x1, waiting for transfers between devices: 5.33 us -> 0.01 us  [route_experts(): lax.all_to_all(own_cols, 'ep', split_axis=0, concat_axis=0, tiled=True)]
    all_to_all x1, waiting for transfers between devices: 1.95 us -> 7.14 us  [route_experts(): lax.all_to_all(reduced, 'ep', split_axis=0, concat_axis=0, tiled=True)]
  transfers between devices with their start and end apart: 4 -> 3, of which waited for: 3 -> 1; matrix products, arithmetic and copies ran while one was open for 3% -> 3% of each run, Pallas kernels for 0% -> 0%
where the time goes in v1:
time: 167 us; the launch traced here: 166 us
  blocking collectives  109 us (65%)
  matrix products  15.3 us (9%)
  between operations  14.5 us (9%)
  starting transfers between devices  10.2 us (6%)
  waiting for transfers between devices  7.18 us (4%)
  other arithmetic  5.35 us (3%)
  local copies, waits for them, and re-layouts  5.11 us (3%)
    unnamed x1, blocking collectives  50.6 us
    all_gather x1, blocking collectives, side_branch(): row_piece = lax.all_gather(after_mixer, 'ep', axis=0, tiled=True)  32.2 us
    all_gather x1, blocking collectives, per_device(): lax.all_gather(partial_value.astype(jnp.bfloat16), 'tp')  7.26 us
    all_to_all x1, waiting for transfers between devices, route_experts(): lax.all_to_all(reduced, 'ep', split_axis=0, concat_axis=0, tiled=True)  7.14 us
    all_gather x1, blocking collectives, route_experts(): whole_rows = lax.all_gather(arrived, 'tp', axis=3, tiled=True)  6.9 us
    all_gather x1, blocking collectives, route_experts(): returned = lax.all_gather(came_back, 'tp', axis=3, tiled=True)  6.34 us
    all_to_all x1, starting transfers between devices, route_experts(): lax.all_to_all(own_cols, 'ep', split_axis=0, concat_axis=0, tiled=True)  5.81 us
    all_gather x1, blocking collectives, side_branch(): lax.all_gather(own_rows.astype(jnp.bfloat16), 'tp', axis=0, tiled=True)  5.24 us
  transfers between devices with their start and end apart: 3, of which 1 were waited for; matrix products, arithmetic and copies ran while one was open for 3% of the time, Pallas kernels for 0%

profile of v1, /device:TPU:0, one launch (start us, length us, event | category | flops | bytes accessed | tf_op | source)
XLA Modules:
  0.0 166.1 jit_solution(11333081261399331628)
XLA Ops:
  7.2 1.6 convolution_multiply_fusion.2
  8.9 0.7 convert_element_type.63
  9.5 1.5 fusion.43
  11.1 0.2 fusion.44
  11.4 0.1 multiply_cosine_fusion
  11.5 0.1 multiply_subtract_fusion
  11.6 0.1 pad_maximum_fusion
  11.7 2.0 %multiply_add_fusion = f32[16,2,128,128]{3,2,1,0:T(8,128)S(1)} fusion(f32[16,2,128,128]{3,2,1,0:T(8,128)} %param.25, f32[16,2,128]{2,1,0:T(2,128)S(1)} %mul.268, f32[16,2,128]{2,1,0:T(2,128)S(1)} %get-tuple-element.13, f32[2]{0:T(128)S(1)} %exponential_subtract_fusion), kind=kLoop, calls=%fused_computation.5 | loop fusion | flops 1572864 | bytes 4227080 | tf_op jit(solution)/shard_map/add | solution.py:157
  13.7 1.9 %fusion.45 = f32[16,2,1,128]{3,2,1,0:T(1,128)S(1)} fusion(f32[16,2,128,1]{2,3,1,0:T(1,128)S(1)} %bitcast.83, f32[16,2,128,128]{3,2,1,0:T(8,128)S(1)} %multiply_add_fusion), kind=kOutput, calls=%fused_computation.85 | convolution fusion | flops 6291456 | bytes 2129920 | tf_op jit(solution)/shard_map/thi,thij->thj/dot_general | solution.py:159
  15.6 0.1 reduce_sum.84
  15.7 0.2 multiply_reduce_fusion.2
  15.9 0.1 multiply_multiply_fusion
  16.0 2.3 %convolution_convert_fusion.2 = bf16[16,2048]{1,0:T(8,128)(2,1)S(1)} fusion(bf16[256,2048]{1,0:T(8,128)(2,1)} %param.31, f32[2,8,2,128]{3,2,1,0:T(2,128)S(1)} %bitcast.82, bf16[16,2048]{1,0:T(8,128)(2,1)S(1)} %copy-done.2, bf16[2048,256]{1,0:T(8,128)(2,1)} %param.29), kind=kOutput, calls=%fused_computation.4 | convolution fusion | flops 33611776 | bytes 2244608 | tf_op jit(solution)/shard_map/dot_general | solution.py:164
  18.3 7.3 %all-gather = bf16[64,2048]{1,0:T(8,128)(2,1)S(1)} all-gather(bf16[16,2048]{1,0:T(8,128)(2,1)S(1)} %convolution_convert_fusion.2), channel_id=2, replica_groups=mesh['ep'=8,'tp'=4] {'tp'}, dimensions={0}, use_global_device_ids=true | all-gather | bytes 327680 | tf_op jit(solution)/shard_map/all_gather | solution.py:165
  25.6 0.1 fusion.20
  25.7 0.2 multiply_reduce_fusion.1
  26.0 0.1 multiply_convert_fusion.1
  26.1 0.1 reshape.167
  26.4 0.1 reshape.166
  26.6 0.1 reduce_window_sum.11
  26.7 0.2 select_reduce_fusion
  26.9 0.3 convolution_convert_fusion
  27.2 0.9 reshape.168
  28.1 0.9 constant_dynamic-slice_fusion
  29.0 0.7 copy.36
  29.8 5.8 %all-to-all-start = ((bf16[8,2,7,512]{3,1,2,0:T(2,128)(2,1)}), bf16[8,2,7,512]{3,1,2,0:T(2,128)(2,1)S(1)}, u32[]{:S(2)}, u32[]{:S(2)}) async-start(bf16[8,2,7,512]{3,1,2,0:T(2,128)(2,1)} %copy.36), calls=%async_computation | async-start | bytes 229376 | tf_op jit(solution)/shard_map/all_to_all | solution.py:68
  35.6 32.2 %all_gather.22 = bf16[128,2048]{1,0:T(8,128)(2,1)S(1)} all-gather(bf16[16,2048]{1,0:T(8,128)(2,1)S(1)} %multiply_convert_fusion.1), channel_id=1, replica_groups=mesh['ep'=8,'tp'=4] {'ep'}, dimensions={0}, use_global_device_ids=true | all-gather | bytes 589824 | tf_op jit(solution)/shard_map/all_gather | solution.py:84
  67.9 0.3 fusion.46
  68.2 0.2 fusion.15
  68.4 1.6 fusion.7
  70.1 0.2 fusion.47
  70.3 6.9 %all_gather.20 = bf16[8,2,7,2048]{3,0,2,1:T(8,128)(2,1)S(1)} all-gather(bf16[8,2,7,512]{3,0,2,1:T(8,128)(2,1)S(1)} %copy.37), channel_id=1, replica_groups=mesh['ep'=8,'tp'=4] {'tp'}, dimensions={3}, use_global_device_ids=true | all-gather | bytes 573440 | tf_op jit(solution)/shard_map/all_gather | solution.py:69
  77.2 1.5 convolution_bitcast_fusion.1
  78.8 1.3 fusion
  80.1 0.2 fusion.11
  80.3 1.8 %fusion.1 = f32[128,2048]{1,0:T(8,128)S(1)} fusion(bf16[128,2048]{1,0:T(8,128)(2,1)} %param.40, bf16[256,2048]{1,0:T(8,128)(2,1)} %param.44, bf16[128,128]{1,0:T(8,128)(2,1)S(1)} %fusion.11, bf16[128,256]{1,0:T(8,128)(2,1)S(1)} %fusion.7), kind=kOutput, calls=%fused_computation.6 | convolution fusion | flops 204668928 | bytes 2719744 | tf_op jit(solution)/shard_map/dot_general | solution.py:103
  82.2 50.6 %all-reduce.2 = bf16[128,2048]{1,0:T(8,128)(2,1)S(1)} all-reduce(f32[128,2048]{1,0:T(8,128)S(1)} %fusion.1), channel_id=4, replica_groups=mesh['ep'=8,'tp'=4] {'ep','tp'}, use_global_device_ids=true, to_apply=%region_9.10.clone | all-reduce | flops 262144 | bytes 1572864
  132.8 5.2 %all-gather.1 = bf16[4,4,2048]{2,1,0:T(4,128)(2,1)S(1)} all-gather(bf16[1,4,2048]{2,1,0:T(4,128)(2,1)S(1)} %fusion.33), channel_id=1, replica_groups=mesh['ep'=8,'tp'=4] {'tp'}, dimensions={0}, use_global_device_ids=true | all-gather | bytes 81920 | tf_op jit(solution)/shard_map/all_gather | solution.py:108
  138.1 1.6 copy.38
  139.7 4.3 %all-to-all-start.1 = ((bf16[8,2,7,512]{3,1,2,0:T(2,128)(2,1)}), bf16[8,2,7,512]{3,1,2,0:T(2,128)(2,1)S(1)}, u32[]{:S(2)}, u32[]{:S(2)}) async-start(bf16[8,2,7,512]{3,1,2,0:T(2,128)(2,1)} %copy.38), calls=%async_computation.2 | async-start | bytes 229376 | tf_op jit(solution)/shard_map/all_to_all | solution.py:72
  144.1 7.1 %all-to-all-done.1 = bf16[8,2,7,512]{3,1,2,0:T(2,128)(2,1)S(1)} async-done(((bf16[8,2,7,512]{3,1,2,0:T(2,128)(2,1)}), bf16[8,2,7,512]{3,1,2,0:T(2,128)(2,1)S(1)}, u32[]{:S(2)}, u32[]{:S(2)}) %all-to-all-start.1) | async-done | bytes 114720 | tf_op jit(solution)/shard_map/all_to_all | solution.py:72
  151.3 6.3 %all_gather.21 = bf16[8,2,7,2048]{3,1,2,0:T(2,128)(2,1)S(1)} all-gather(bf16[8,2,7,512]{3,1,2,0:T(2,128)(2,1)S(1)} %all-to-all-done.1), channel_id=1, replica_groups=mesh['ep'=8,'tp'=4] {'tp'}, dimensions={3}, use_global_device_ids=true | all-gather | bytes 573440 | tf_op jit(solution)/shard_map/all_gather | solution.py:73
  157.6 0.2 copy.39
  157.8 0.2 reshape.179
  157.9 0.3 fusion.5
  158.2 0.1 fusion.40
  158.4 0.2 multiply_reduce_fusion
  158.6 0.7 multiply_convert_fusion
  (55 shorter events, 0.7 us)
Async XLA Ops:
  7.2 71.6 %copy-start = (bf16[2,128,2048]{2,1,0:T(8,128)(2,1)S(1)}, bf16[2,128,2048]{2,1,0:T(8,128)(2,1)}, u32[]{:S(2)}) copy-start(bf16[2,128,2048]{2,1,0:T(8,128)(2,1)} %param.37) | copy-start | bytes 3145732
  7.2 3.9 %copy-start.2 = (bf16[16,2048]{1,0:T(8,128)(2,1)S(1)}, bf16[16,2048]{1,0:T(8,128)(2,1)}, u32[]{:S(2)}) copy-start(bf16[16,2048]{1,0:T(8,128)(2,1)} %param.23) | copy-start | bytes 196612
  7.2 3.9 %copy-start.4 = (bf16[2048,256]{1,0:T(8,128)(2,1)S(1)}, bf16[2048,256]{1,0:T(8,128)(2,1)}, u32[]{:S(2)}) copy-start(bf16[2048,256]{1,0:T(8,128)(2,1)} %param.28) | copy-start | bytes 3145732
  13.7 4.6 %copy-start.1 = (f32[16,2,128,128]{3,2,1,0:T(8,128)}, f32[16,2,128,128]{3,2,1,0:T(8,128)S(1)}, u32[]{:S(2)}) copy-start(f32[16,2,128,128]{3,2,1,0:T(8,128)S(1)} %multiply_add_fusion) | copy-start | bytes 6291460
  13.7 2.2 %copy-start.12 = (f32[256]{0:T(256)S(1)}, f32[256]{0:T(256)}, u32[]{:S(2)}) copy-start(f32[256]{0:T(256)} %param.30) | copy-start | bytes 3076
  15.6 10.4 %copy-start.8 = (f32[2048]{0:T(1024)S(1)}, f32[2048]{0:T(1024)}, u32[]{:S(2)}) copy-start(f32[2048]{0:T(1024)} %param.32) | copy-start | bytes 24580
  16.0 10.3 %copy-start.10 = (s32[16,6]{0,1:T(8,128)S(1)}, s32[16,6]{0,1:T(8,128)}, u32[]{:S(2)}) copy-start(s32[16,6]{0,1:T(8,128)} %param.33) | copy-start | bytes 1156
  26.1 41.7 %copy-start.11 = (bf16[2048]{0:T(1024)(128)(2,1)S(1)}, bf16[2048]{0:T(1024)(128)(2,1)}, u32[]{:S(2)}) copy-start(bf16[2048]{0:T(1024)(128)(2,1)} %param.41) | copy-start | bytes 12292
  26.1 41.7 %copy-start.5 = (bf16[2048,256]{1,0:T(8,128)(2,1)S(1)}, bf16[2048,256]{1,0:T(8,128)(2,1)}, u32[]{:S(2)}) copy-start(bf16[2048,256]{1,0:T(8,128)(2,1)} %param.42) | copy-start | bytes 3145732
  29.8 40.5 %all-to-all-start = ((bf16[8,2,7,512]{3,1,2,0:T(2,128)(2,1)}), bf16[8,2,7,512]{3,1,2,0:T(2,128)(2,1)S(1)}, u32[]{:S(2)}, u32[]{:S(2)}) async-start(bf16[8,2,7,512]{3,1,2,0:T(2,128)(2,1)} %copy.36), calls=%async_computation | async-start | bytes 229376 | tf_op jit(solution)/shard_map/all_to_all | solution.py:68
  35.6 102.5 %reduce-scatter.2.cloned.1.call-start = ((), (), s32[]{:S(2)}) async-start(), calls=%async_computation.3 | async-start | bytes 573440 | tf_op jit(solution)/shard_map/reduce_scatter | solution.py:71
  68.2 1.9 %copy-start.6 = (bf16[2048,128]{1,0:T(8,128)(2,1)S(1)}, bf16[2048,128]{1,0:T(8,128)(2,1)}, u32[]{:S(2)}) copy-start(bf16[2048,128]{1,0:T(8,128)(2,1)} %param.38) | copy-start | bytes 1572868
  68.4 10.3 %copy-start.3 = (bf16[2,2048,128]{2,1,0:T(8,128)(2,1)S(1)}, bf16[2,2048,128]{2,1,0:T(8,128)(2,1)}, u32[]{:S(2)}) copy-start(bf16[2,2048,128]{2,1,0:T(8,128)(2,1)} %param.36) | copy-start | bytes 3145732
  78.8 1.3 copy-start.7
  82.1 75.8 %copy-start.13 = (f32[16,6]{0,1:T(8,128)S(1)}, f32[16,6]{0,1:T(8,128)}, u32[]{:S(2)}) copy-start(f32[16,6]{0,1:T(8,128)} %param.34) | copy-start | bytes 1156
  138.0 20.6 %copy-start.9 = (f32[2048]{0:T(1024)S(1)}, f32[2048]{0:T(1024)}, u32[]{:S(2)}) copy-start(f32[2048]{0:T(1024)} %param.45) | copy-start | bytes 24580
  139.7 11.6 %all-to-all-start.1 = ((bf16[8,2,7,512]{3,1,2,0:T(2,128)(2,1)}), bf16[8,2,7,512]{3,1,2,0:T(2,128)(2,1)S(1)}, u32[]{:S(2)}, u32[]{:S(2)}) async-start(bf16[8,2,7,512]{3,1,2,0:T(2,128)(2,1)} %copy.38), calls=%async_computation.2 | async-start | bytes 229376 | tf_op jit(solution)/shard_map/all_to_all | solution.py:72
Sparse Core Ops, SparseCore 0:
  80.2 21.2 reduce-scatter.1
